TPU v7x, 32 devices: a whole 2x2x4 slice. The times are simulated.
32 devices in a mesh: ep: 4 (over y, x), tp: 8 (over z, core).
Axes of the slice: x: 2, y: 2, z: 4, core: 2. Of those that a mesh axis runs over, the one named last changes fastest.
Arguments:
- tokens: bfloat16 [256, 2048], P('ep', 'tp'), may hold values from -64 to 64
- mixer_gain: float32 [2048], replicated, may hold values from 0.1 to 1.9
- expert_gain: float32 [2048], replicated, may hold values from 0.1 to 1.9
- query_weight: bfloat16 [2048, 1024], P(None, 'tp'), may hold values from -0.125 to 0.125
- key_weight: bfloat16 [2048, 1024], P(None, 'tp'), may hold values from -0.125 to 0.125
- value_weight: bfloat16 [2048, 4, 256], P(None, None, 'tp'), may hold values from -0.125 to 0.125
- outgate_weight: bfloat16 [2048, 4, 256], P(None, None, 'tp'), may hold values from -0.125 to 0.125
- ingate_weight: bfloat16 [2048, 4], replicated, may hold values from -0.125 to 0.125
- forget_weight: bfloat16 [2048, 4], replicated, may hold values from -0.125 to 0.125
- forget_bias: float32 [4], replicated, may hold values from -1 to 4
- mixout_weight: bfloat16 [1024, 2048], replicated, may hold values from -0.1875 to 0.1875
- memory_state: float32 [256, 4, 256, 256], P('ep', None, 'tp'), may hold values from -0.6 to 0.6
- norm_state: float32 [256, 4, 256], P('ep'), may hold values from -0.6 to 0.6
- max_state: float32 [256, 4], P('ep'), may hold values from -4 to 4
- expert_gate: bfloat16 [64, 2048, 256], P(('ep', 'tp')), may hold values from -0.125 to 0.125
- expert_up: bfloat16 [64, 2048, 256], P(('ep', 'tp')), may hold values from -0.125 to 0.125
- expert_down: bfloat16 [64, 256, 2048], P(('ep', 'tp')), may hold values from -0.1875 to 0.1875
- routes: int32 [256, 2], P('ep'), may hold values from 0 to 15, all different within a row; in each aligned block of 64 rows (0 to 63, 64 to 127, ...) at most 16 rows name the same one
- route_weights: float32 [256, 2], P('ep'), may hold values from 0.1 to 1
Outputs:
- mixed_out: bfloat16 [256, 2048], P('ep', 'tp')
- memory_next: float32 [256, 4, 256, 256], P('ep', None, 'tp')
- norm_next: float32 [256, 4, 256], P('ep')
- max_next: float32 [256, 4], P('ep')
Inputs may be any that keep to these rules, and one draw needn't show every extreme that they name: `routes`: each row names 2 different experts; in the rows of one index of ep (aligned blocks of 64 rows) no expert is named by more than 16 rows, a bound that some block reaches.
All inputs are finite; a program needn't handle non-finite values.
Results may differ from a plain program's by a relative error of at most 0.0079.
Values may be sent and summed in bfloat16 or wider, within the bound.
A program may use at most 64 MiB of HBM per device.

v0:
```python
import jax
import jax.numpy as jnp
from jax import lax
from jax.sharding import PartitionSpec as P

FF_SPLIT = 4


eps = 1e-06


def rms_inverse(row_float):
    return lax.rsqrt(jnp.mean(row_float * row_float, axis=1, keepdims=True) + eps)


def slot_targets(routes, expert_count, capacity):
    flat_routes = routes.reshape(-1)
    onehot = (flat_routes[:, None] == jnp.arange(expert_count, dtype=jnp.int32)[None, :]).astype(
        jnp.int32
    )
    counts = jnp.cumsum(onehot, axis=0)
    slot_rank = jnp.sum(onehot * (counts - 1), axis=1)
    return flat_routes * capacity + slot_rank


def local(
    tokens,
    mixer_gain,
    expert_gain,
    query_weight,
    key_weight,
    value_weight,
    outgate_weight,
    ingate_weight,
    forget_weight,
    forget_bias,
    mixout_weight,
    memory_state,
    norm_state,
    max_state,
    expert_gate,
    expert_up,
    expert_down,
    routes,
    route_weights,
):
    seq_count, own_width = tokens.shape
    model_width = mixer_gain.shape[0]
    head_count = ingate_weight.shape[1]
    head_dim = norm_state.shape[2]
    local_values = value_weight.shape[2]
    offset = lax.axis_index("tp") * own_width
    full_rows = lax.all_gather(tokens, "tp", axis=1, tiled=True)
    full_float = full_rows.astype(jnp.float32)
    inverse = rms_inverse(full_float)
    scaled = (full_float * mixer_gain).astype(jnp.bfloat16)
    query_own = inverse * jnp.dot(scaled, query_weight, preferred_element_type=jnp.float32)
    key_own = (
        inverse
        * jnp.dot(scaled, key_weight, preferred_element_type=jnp.float32)
        * head_dim ** (-0.5)
    )
    query_cols, key_cols = (
        lax.all_gather(query_own, "tp", axis=1, tiled=True),
        lax.all_gather(key_own, "tp", axis=1, tiled=True),
    )
    query_full = query_cols.reshape(seq_count, head_count, head_dim)
    key_full = key_cols.reshape(seq_count, head_count, head_dim)
    values = (
        inverse
        * jnp.dot(
            scaled,
            value_weight.reshape(model_width, head_count * local_values),
            preferred_element_type=jnp.float32,
        )
    ).reshape(seq_count, head_count, local_values)
    outgate = (
        inverse
        * jnp.dot(
            scaled,
            outgate_weight.reshape(model_width, head_count * local_values),
            preferred_element_type=jnp.float32,
        )
    ).reshape(seq_count, head_count, local_values)
    ingate = inverse * jnp.dot(scaled, ingate_weight, preferred_element_type=jnp.float32)
    logforget = jax.nn.log_sigmoid(
        inverse * jnp.dot(scaled, forget_weight, preferred_element_type=jnp.float32) + forget_bias
    )
    max_next = jnp.maximum(logforget + max_state, ingate)
    decay_rate = jnp.exp(logforget + max_state - max_next)
    inflow = jnp.exp(ingate - max_next)
    memory_next = (
        decay_rate[:, :, None, None] * memory_state
        + inflow[:, :, None, None] * values[:, :, :, None] * key_full[:, :, None, :]
    )
    norm_next = decay_rate[:, :, None] * norm_state + inflow[:, :, None] * key_full
    numerator = jnp.einsum(
        "shvk,shk->shv", memory_next, query_full, precision=lax.Precision.HIGHEST
    )
    denominator = jnp.maximum(jnp.abs(jnp.sum(norm_next * query_full, axis=2)), jnp.exp(-max_next))
    gated_heads = (jax.nn.sigmoid(outgate) * (numerator / denominator[:, :, None])).astype(
        jnp.bfloat16
    )
    heads_full = lax.all_gather(gated_heads, "tp", axis=2, tiled=True).reshape(
        seq_count, head_count * head_dim
    )
    group_count = lax.axis_size("ep")
    width_count = lax.axis_size("tp")
    block_count = expert_gate.shape[0]
    local_experts = block_count * width_count // FF_SPLIT
    expert_count = local_experts * group_count
    topk_count = routes.shape[1]
    capacity = max(2, 2 * seq_count * topk_count // expert_count)
    slot_count = expert_count * capacity
    targets = slot_targets(routes, expert_count, capacity)
    slot_iota = jnp.arange(slot_count, dtype=jnp.int32)
    picker = (
        (targets[:, None] == slot_iota[None, :])
        .astype(jnp.bfloat16)
        .reshape(seq_count, topk_count, slot_count)
        .sum(axis=1)
    )
    middle_full = (
        full_float + jnp.dot(heads_full, mixout_weight, preferred_element_type=jnp.float32)
    ).astype(jnp.bfloat16)
    middle_own = lax.dynamic_slice_in_dim(middle_full, offset, own_width, 1)
    middle_float = middle_full.astype(jnp.float32)
    normed_full = (middle_float * rms_inverse(middle_float) * expert_gain).astype(jnp.bfloat16)
    buffer = jnp.einsum(
        "sr,sd->rd", picker, normed_full, preferred_element_type=jnp.float32
    ).astype(jnp.bfloat16)
    expert_rows = lax.all_to_all(
        buffer.reshape(group_count, local_experts * capacity, normed_full.shape[1]),
        "ep",
        split_axis=0,
        concat_axis=0,
        tiled=True,
    )
    row_block = expert_rows.reshape(group_count, local_experts, capacity, model_width)
    block_expert = (
        lax.axis_index("tp") * block_count + jnp.arange(block_count, dtype=jnp.int32)
    ) // FF_SPLIT
    block_rows = jnp.take(row_block, block_expert, axis=1)
    gate_part = jnp.einsum(
        "glcd,ldf->glcf", block_rows, expert_gate, preferred_element_type=jnp.float32
    )
    up_part = jnp.einsum(
        "glcd,ldf->glcf", block_rows, expert_up, preferred_element_type=jnp.float32
    )
    hidden = (jax.nn.silu(gate_part) * up_part).astype(jnp.bfloat16)
    down_part = jnp.einsum(
        "glcf,lfd->glcd", hidden, expert_down, preferred_element_type=jnp.float32
    )
    owner = (block_expert[:, None] == jnp.arange(local_experts, dtype=jnp.int32)[None, :]).astype(
        jnp.float32
    )
    term = jnp.einsum("glcd,le->gecd", down_part, owner, precision=lax.Precision.HIGHEST).reshape(
        group_count, local_experts * capacity, model_width
    )
    down_share = lax.psum_scatter(term, "tp", scatter_dimension=2, tiled=True)
    outgoing = down_share.astype(jnp.bfloat16)
    returned = lax.all_to_all(outgoing, "ep", split_axis=0, concat_axis=0, tiled=True).reshape(
        slot_count, own_width
    )
    shares = route_weights / jnp.sum(route_weights, axis=1, keepdims=True)
    matches = (
        targets.reshape(seq_count, topk_count)[:, :, None] == slot_iota[None, None, :]
    ).astype(jnp.float32)
    combiner = jnp.sum(matches * shares[:, :, None], axis=1)
    expert_sum = jnp.dot(combiner, returned.astype(jnp.float32), precision=lax.Precision.HIGHEST)
    mixed_out = (middle_own.astype(jnp.float32) + expert_sum).astype(jnp.bfloat16)
    return (mixed_out, memory_next, norm_next, max_next)


def solution(mesh):
    in_specs = (
        P("ep", "tp"),
        P(),
        P(),
        P(None, "tp"),
        P(None, "tp"),
        P(None, None, "tp"),
        P(None, None, "tp"),
        P(),
        P(),
        P(),
        P(),
        P("ep", None, "tp", None),
        P("ep", None, None),
        P("ep", None),
        P(("ep", "tp"), None, None),
        P(("ep", "tp"), None, None),
        P(("ep", "tp"), None, None),
        P("ep", None),
        P("ep", None),
    )
    out_specs = (P("ep", "tp"), P("ep", None, "tp", None), P("ep", None, None), P("ep", None))
    return jax.shard_map(local, mesh=mesh, in_specs=in_specs, out_specs=out_specs, check_vma=False)
```

profile of v0, /device:TPU:0, one launch (start us, length us, event | category | flops | bytes accessed | tf_op | source)
XLA Modules:
  0.0 185.8 jit_solution(12540106460633736876)
XLA Ops:
  7.2 16.3 %all_gather.12 = bf16[64,2048]{1,0:T(8,128)(2,1)S(1)} all-gather(bf16[64,256]{1,0:T(8,128)(2,1)} %param.19), channel_id=1, replica_groups=mesh['ep'=4,'tp'=8] {'tp'}, dimensions={1}, use_global_device_ids=true | all-gather | bytes 294912 | tf_op jit(solution)/shard_map/all_gather | solution.py:53
  23.7 1.3 convolution_multiply_fusion
  24.9 14.2 %all_gather.14 = f32[64,1024]{1,0:T(8,128)S(1)} all-gather(f32[64,128]{1,0:T(8,128)S(1)} %convolution_multiply_fusion), channel_id=1, replica_groups=mesh['ep'=4,'tp'=8] {'tp'}, dimensions={1}, use_global_device_ids=true | all-gather | bytes 294912 | tf_op jit(solution)/shard_map/all_gather | solution.py:64
  40.0 1.3 convolution_multiply_fusion.2
  44.3 14.2 %all_gather.13 = f32[64,1024]{1,0:T(8,128)S(1)} all-gather(f32[64,128]{1,0:T(8,128)S(1)} %fusion.21), channel_id=1, replica_groups=mesh['ep'=4,'tp'=8] {'tp'}, dimensions={1}, use_global_device_ids=true | all-gather | bytes 294912 | tf_op jit(solution)/shard_map/all_gather | solution.py:65
  58.7 4.9 %multiply_add_fusion = f32[64,4,32,256]{3,2,1,0:T(8,128)S(1)} fusion(f32[64,4,32,256]{3,2,1,0:T(8,128)} %param.30, f32[64,4,256]{2,1,0:T(4,128)S(1)} %mul.187, f32[64,4,32]{2,1,0:T(4,128)S(1)} %copy.72, f32[64,4]{1,0:T(8,128)} %copy.70), kind=kLoop, calls=%fused_computation.1 | loop fusion | flops 6291456 | bytes 17073152 | tf_op jit(solution)/shard_map/add | solution.py:93
  63.6 3.4 %copy-done.1 = f32[64,4,32,256]{3,2,1,0:T(8,128)} copy-done((f32[64,4,32,256]{3,2,1,0:T(8,128)}, f32[64,4,32,256]{3,2,1,0:T(8,128)S(1)}, u32[]{:S(2)}) %copy-start.1) | copy-done | bytes 8388632
  67.0 7.3 %fusion.70 = f32[64,4,1,32]{3,2,1,0:T(1,128)S(1)} fusion(f32[64,4,32,256]{3,2,1,0:T(8,128)S(1)} %multiply_add_fusion, f32[64,4,256,1]{2,3,1,0:T(1,128)S(1)} %reshape.192), kind=kOutput, calls=%fused_computation.95 | convolution fusion | flops 25165824 | bytes 8683520 | tf_op jit(solution)/shard_map/shvk,shk->shv/dot_general | solution.py:97
  74.4 1.9 %multiply_reduce_fusion = (f32[64,4]{1,0:T(8,128)S(1)}, f32[64,4,256]{2,1,0:T(4,128)}) fusion(f32[64,4,256]{2,1,0:T(4,128)S(1)} %reshape.171, f32[64,4,256]{2,1,0:T(4,128)S(1)} %mul.187, f32[64,4]{1,0:T(8,128)S(1)} %copy-done.4, f32[64,4,256]{2,1,0:T(4,128)} %param.31, f32[64,4]{1,0:T(8,128)S(1)} %copy-done.3), kind=kLoop, calls=%fused_computation.46 | loop fusion | flops 327424 | bytes 1051648 | tf_op jit(solution)/shard_map/reduce_sum | solution.py:100
  76.3 1.4 fusion.25
  77.8 14.4 %all_gather.15 = bf16[64,4,256]{0,2,1:T(8,128)(2,1)S(1)} all-gather(bf16[64,4,32]{0,2,1:T(8,128)(2,1)S(1)} %fusion.54), channel_id=1, replica_groups=mesh['ep'=4,'tp'=8] {'tp'}, dimensions={2}, use_global_device_ids=true | all-gather | bytes 147456 | tf_op jit(solution)/shard_map/all_gather | solution.py:104
  92.3 3.2 %fusion.29 = (f32[64]{0:T(128)S(1)}, bf16[64,2048]{1,0:T(8,128)(2,1)S(1)}) fusion(bf16[64,1024]{0,1:T(8,128)(2,1)S(1)} %bitcast.82, bf16[1024,2048]{1,0:T(8,128)(2,1)} %param.29, bf16[64,2048]{1,0:T(8,128)(2,1)S(1)} %all_gather.12), kind=kOutput, calls=%fused_computation.36 | convolution fusion | flops 269221824 | bytes 4849920 | tf_op jit(solution)/shard_map/dot_general | solution.py:124
  96.5 1.5 convolution_convert_fusion
  98.0 3.7 %all-to-all-start = ((bf16[4,64,2048]{2,1,0:T(8,128)(2,1)}), bf16[4,64,2048]{2,1,0:T(8,128)(2,1)S(1)}, u32[]{:S(2)}, u32[]{:S(2)}) async-start(bf16[4,64,2048]{2,1,0:T(8,128)(2,1)} %bitcast.8), calls=%async_computation | async-start | bytes 2097152 | tf_op jit(solution)/shard_map/all_to_all | solution.py:132
  101.8 14.2 %all-to-all-done = bf16[4,64,2048]{2,1,0:T(8,128)(2,1)S(1)} async-done(((bf16[4,64,2048]{2,1,0:T(8,128)(2,1)}), bf16[4,64,2048]{2,1,0:T(8,128)(2,1)S(1)}, u32[]{:S(2)}, u32[]{:S(2)}) %all-to-all-start) | async-done | bytes 1048608 | tf_op jit(solution)/shard_map/all_to_all | solution.py:132
  116.9 1.8 gather_fusion
  118.7 2.1 %fusion.6 = f32[4,2,16,256]{3,2,0,1:T(8,128)S(1)} fusion(bf16[2,2048,256]{2,1,0:T(8,128)(2,1)} %param.33, bf16[2,4,16,2048]{3,2,1,0:T(8,128)(2,1)S(1)} %gather_fusion, pred[2]{0:T(512)(128)(4,1)S(1)} %compare_and_fusion), kind=kOutput, calls=%fused_computation.12 | convolution fusion | flops 134479872 | bytes 2752514 | tf_op jit(solution)/shard_map/glcd,ldf->glcf/dot_general | solution.py:144
  120.8 3.5 %convolution_bitcast_fusion.1 = f32[4,2,16,2048]{3,2,0,1:T(8,128)} fusion(bf16[2,256,2048]{2,1,0:T(8,128)(2,1)S(1)} %copy-done, bf16[2,2048,256]{2,1,0:T(8,128)(2,1)} %param.34, bf16[2,4,16,2048]{3,2,1,0:T(8,128)(2,1)S(1)} %gather_fusion, pred[2]{0:T(512)(128)(4,1)S(1)} %compare_and_fusion, f32[4,2,16,256]{3,2,0,1:T(8,128)S(1)} %fusion.6), kind=kOutput, calls=%fused_computation.4 | convolution fusion | flops 268894208 | bytes 5898242 | tf_op jit(solution)/shard_map/glcf,lfd->glcd/dot_general | solution.py:151
  124.4 4.6 %convolution_bitcast_fusion = f32[4,4,16,2048]{3,1,2,0:T(4,128)S(1)} fusion(f32[4,2,16,2048]{3,2,0,1:T(8,128)} %convolution_bitcast_fusion.1, s32[2]{0:T(128)S(1)} %and_select_fusion.1), kind=kOutput, calls=%fused_computation.2 | convolution fusion | flops 12582920 | bytes 3145736 | tf_op jit(solution)/shard_map/glcd,le->gecd/dot_general | solution.py:157
  129.0 2.6 %copy.79 = f32[4,4,16,2048]{3,2,1,0:T(8,128)} copy(f32[4,4,16,2048]{3,1,2,0:T(4,128)S(1)} %convolution_bitcast_fusion) | data formatting | bytes 4194304 | tf_op jit(solution)/shard_map/glcd,le->gecd/transpose | solution.py:157
  132.3 35.6 %reduce-scatter.2.cloned.1.call-done = f32[4,64,256]{2,1,0:T(8,128)} async-done(((f32[4,64,2048]{2,1,0:T(8,128)}), f32[4,64,256]{2,1,0:T(8,128)}) %reduce-scatter.2.cloned.1.call-update) | async-done | bytes 262160 | tf_op jit(solution)/shard_map/reduce_scatter | solution.py:160
  167.9 1.6 convert_element_type.56
  169.5 3.6 %all-to-all-start.1 = ((bf16[4,64,256]{2,1,0:T(8,128)(2,1)}), bf16[4,64,256]{2,1,0:T(8,128)(2,1)S(1)}, u32[]{:S(2)}, u32[]{:S(2)}) async-start(bf16[4,64,256]{2,1,0:T(8,128)(2,1)} %convert_element_type.56), calls=%async_computation.2 | async-start | bytes 262144 | tf_op jit(solution)/shard_map/all_to_all | solution.py:162
  173.2 4.9 %all-to-all-done.1 = bf16[4,64,256]{2,1,0:T(8,128)(2,1)S(1)} async-done(((bf16[4,64,256]{2,1,0:T(8,128)(2,1)}), bf16[4,64,256]{2,1,0:T(8,128)(2,1)S(1)}, u32[]{:S(2)}, u32[]{:S(2)}) %all-to-all-start.1) | async-done | bytes 131104 | tf_op jit(solution)/shard_map/all_to_all | solution.py:162
  (66 shorter events, 8.0 us)
Async XLA Ops:
  7.2 113.7 %copy-start = (bf16[2,256,2048]{2,1,0:T(8,128)(2,1)S(1)}, bf16[2,256,2048]{2,1,0:T(8,128)(2,1)}, u32[]{:S(2)}) copy-start(bf16[2,256,2048]{2,1,0:T(8,128)(2,1)} %param.35) | copy-start | bytes 6291460
  7.2 32.4 %copy-start.5 = (f32[2048]{0:T(1024)S(1)}, f32[2048]{0:T(1024)}, u32[]{:S(2)}) copy-start(f32[2048]{0:T(1024)} %param.20) | copy-start | bytes 24580
  7.2 32.4 %copy-start.10 = (bf16[2048,4]{0,1:T(4,128)(2,1)S(1)}, bf16[2048,4]{0,1:T(4,128)(2,1)}, u32[]{:S(2)}) copy-start(bf16[2048,4]{0,1:T(4,128)(2,1)} %param.26) | copy-start | bytes 49156
  7.2 32.6 %copy-start.11 = (bf16[2048,4]{0,1:T(4,128)(2,1)S(1)}, bf16[2048,4]{0,1:T(4,128)(2,1)}, u32[]{:S(2)}) copy-start(bf16[2048,4]{0,1:T(4,128)(2,1)} %param.27) | copy-start | bytes 49156
  7.2 32.6 %copy-start.13 = (f32[4]{0:T(128)S(1)}, f32[4]{0:T(128)}, u32[]{:S(2)}) copy-start(f32[4]{0:T(128)} %param.28) | copy-start | bytes 52
  7.2 32.6 %copy-start.12 = (f32[64,4]{0,1:T(4,128)S(1)}, f32[64,4]{0,1:T(4,128)}, u32[]{:S(2)}) copy-start(f32[64,4]{0,1:T(4,128)} %param.32) | copy-start | bytes 3076
  40.0 36.3 %copy-start.7 = (f32[64,4]{0,1:T(4,128)}, f32[64,4]{0,1:T(4,128)S(1)}, u32[]{:S(2)}) copy-start(f32[64,4]{0,1:T(4,128)S(1)} %get-tuple-element.7) | copy-start | bytes 3076
  63.6 3.4 %copy-start.1 = (f32[64,4,32,256]{3,2,1,0:T(8,128)}, f32[64,4,32,256]{3,2,1,0:T(8,128)S(1)}, u32[]{:S(2)}) copy-start(f32[64,4,32,256]{3,2,1,0:T(8,128)S(1)} %multiply_add_fusion) | copy-start | bytes 25165828
  67.0 7.4 %copy-start.3 = (f32[64,4]{1,0:T(8,128)S(1)}, f32[64,4]{1,0:T(8,128)}, u32[]{:S(2)}) copy-start(f32[64,4]{1,0:T(8,128)} %copy.70) | copy-start | bytes 3076
  67.0 7.4 %copy-start.4 = (f32[64,4]{1,0:T(8,128)S(1)}, f32[64,4]{1,0:T(8,128)}, u32[]{:S(2)}) copy-start(f32[64,4]{1,0:T(8,128)} %copy.74) | copy-start | bytes 3076
  92.3 3.2 %copy-start.8 = (s32[64,2]{0,1:T(2,128)S(1)}, s32[64,2]{0,1:T(2,128)}, u32[]{:S(2)}) copy-start(s32[64,2]{0,1:T(2,128)} %param.36) | copy-start | bytes 1540
  92.3 4.2 %copy-start.6 = (f32[2048]{0:T(1024)S(1)}, f32[2048]{0:T(1024)}, u32[]{:S(2)}) copy-start(f32[2048]{0:T(1024)} %param.21) | copy-start | bytes 24580
  98.0 17.9 %all-to-all-start = ((bf16[4,64,2048]{2,1,0:T(8,128)(2,1)}), bf16[4,64,2048]{2,1,0:T(8,128)(2,1)S(1)}, u32[]{:S(2)}, u32[]{:S(2)}) async-start(bf16[4,64,2048]{2,1,0:T(8,128)(2,1)} %bitcast.8), calls=%async_computation | async-start | bytes 2097152 | tf_op jit(solution)/shard_map/all_to_all | solution.py:132
  101.7 66.2 %reduce-scatter.2.cloned.1.call-start = ((), (), s32[]{:S(2)}) async-start(), calls=%async_computation.3 | async-start | bytes 2359296 | tf_op jit(solution)/shard_map/reduce_scatter | solution.py:160
  115.9 1.0 copy-start.2
  131.6 0.7 copy-start.9
  169.5 8.6 %all-to-all-start.1 = ((bf16[4,64,256]{2,1,0:T(8,128)(2,1)}), bf16[4,64,256]{2,1,0:T(8,128)(2,1)S(1)}, u32[]{:S(2)}, u32[]{:S(2)}) async-start(bf16[4,64,256]{2,1,0:T(8,128)(2,1)} %convert_element_type.56), calls=%async_computation.2 | async-start | bytes 262144 | tf_op jit(solution)/shard_map/all_to_all | solution.py:162
Sparse Core Ops, SparseCore 0:
  131.7 36.1 reduce-scatter.1
where the time goes:
time: 187 us; the launch traced here: 186 us
  blocking collectives  59.1 us (32%)
  waiting for transfers between devices  54.7 us (29%)
  matrix products  28.7 us (15%)
  between operations  14.4 us (8%)
  local copies, waits for them, and re-layouts  12.3 us (7%)
  other arithmetic  9.31 us (5%)
  starting transfers between devices  7.3 us (4%)
    reduce_scatter x1, waiting for transfers between devices, local(): down_share = lax.psum_scatter(term, 'tp', scatter_dimension=2, tiled=True)  35.6 us
    all_gather x1, blocking collectives, local(): full_rows = lax.all_gather(tokens, 'tp', axis=1, tiled=True)  16.3 us
    all_gather x1, blocking collectives, local(): lax.all_gather(gated_heads, 'tp', axis=2, tiled=True)  14.4 us
    all_gather x1, blocking collectives, local(): lax.all_gather(key_own, 'tp', axis=1, tiled=True)  14.2 us
    all_gather x1, blocking collectives, local(): lax.all_gather(query_own, 'tp', axis=1, tiled=True)  14.2 us
    all_to_all x1, waiting for transfers between devices, local(): lax.all_to_all(buffer.reshape(group_count, local_experts * capacity, norm...  14.2 us
    dot_general x1, matrix products, local(): jnp.einsum('shvk,shk->shv', memory_next, query_full, precision=lax.Precis...  7.28 us
    unnamed x29, local copies, waits for them, and re-layouts  5.2 us
  transfers between devices with their start and end apart: 3, of which 3 were waited for; matrix products, arithmetic and copies ran while one was open for 0% of the time, Pallas kernels for 0%

commit v1 on v0

v1 whole, which is shorter than its diff:
```python
import functools

import jax
import jax.numpy as jnp
from jax import lax
from jax.experimental import pallas as pl
from jax.experimental.pallas import tpu as pltpu
from jax.sharding import PartitionSpec as P

FF_SPLIT = 4
MESH = pl.DeviceIdType.MESH
VMEM = pltpu.VMEM
eps = 1e-06
F32 = jnp.float32
BF16 = jnp.bfloat16
GROUP = 8
TRANS = (((1,), (1,)), ((), ()))


def dot_t(left, right):
    return lax.dot_general(left, right, TRANS, preferred_element_type=F32)


def per_head(columns, head_count, each, width):
    head = lax.broadcasted_iota(jnp.int32, (columns.shape[0], width), 1) // each
    out = jnp.zeros((columns.shape[0], width), F32)
    for h in range(head_count):
        out = jnp.where(head == h, columns[:, h : h + 1], out)
    return out


def send(source, slot, send_sem, recv_sem, other):
    return pltpu.make_async_remote_copy(
        src_ref=source,
        dst_ref=slot,
        send_sem=send_sem,
        recv_sem=recv_sem,
        device_id={"tp": other},
        device_id_type=MESH,
    )


def spread(n, me, source, slots, sems):
    chips, chip, core = n // 2, me // 2, lax.rem(me, 2)
    for d in range(1, chips):
        other = lax.rem(chip + d, chips) * 2 + core
        send(source, slots.at[me], sems.at[0], sems.at[1 + d], other).start()
    send(source, slots.at[me], sems.at[0], sems.at[1], chip * 2 + 1 - core).start()


def relay(n, me, slots, sems):
    chips, chip, core = n // 2, me // 2, lax.rem(me, 2)
    partner = chip * 2 + 1 - core
    for d in range(1, chips):
        held = slots.at[lax.rem(chip + chips - d, chips) * 2 + core]
        send(held, held, sems.at[0], sems.at[1 + d], partner).wait_recv()
        send(held, held, sems.at[0], sems.at[1], partner).start()
    part = slots.at[pl.ds(0, chips)]
    send(part, part, sems.at[0], sems.at[1], partner).wait_recv()


def sent(n, slots, sems):
    part = slots.at[pl.ds(0, n - 1)]
    send(part, part, sems.at[0], sems.at[1], lax.axis_index("tp")).wait_send()


def bytes_wait(part, send_sem, recv_sem, here):
    done = pltpu.make_async_remote_copy(
        src_ref=part,
        dst_ref=part,
        send_sem=send_sem,
        recv_sem=recv_sem,
        device_id=here,
        device_id_type=MESH,
    )
    return done


def project_kernel(
    n,
    head_dim,
    tok,
    gain,
    wq_hbm,
    wk_hbm,
    wv_hbm,
    wo_hbm,
    wi,
    wf,
    bias,
    max_t,
    x_out,
    q_out,
    k_out,
    inflow_values,
    sig_out,
    decay_out,
    inflow_out,
    max_out,
    slots,
    qks,
    wq,
    wk,
    wv,
    wo,
    scaled,
    load_sems,
    sems,
    qk_sems,
):
    me = lax.axis_index("tp")
    loads = [
        pltpu.make_async_copy(a, b, load_sems.at[i])
        for i, (a, b) in enumerate(((wq_hbm, wq), (wk_hbm, wk), (wv_hbm, wv), (wo_hbm, wo)))
    ]
    for one in loads:
        one.start()
    barrier = pltpu.get_barrier_semaphore()
    for d in range(1, n):
        pl.semaphore_signal(
            barrier, inc=1, device_id={"tp": lax.rem(me + d, n)}, device_id_type=MESH
        )
    pl.semaphore_wait(barrier, n - 1)
    spread(n, me, tok, slots, sems)
    slots[me] = tok[...]
    seqs, own = tok.shape
    relay(n, me, slots, sems)
    total = jnp.zeros((seqs, 1), F32)
    for j in range(n):
        part = slots[j].astype(F32)
        x_out[:, j * own : (j + 1) * own] = slots[j]
        total = total + jnp.sum(part * part, axis=1, keepdims=True)
        scaled[:, j * own : (j + 1) * own] = (part * gain[:, j * own : (j + 1) * own]).astype(BF16)
    inverse = lax.rsqrt(total / (n * own) + eps)
    sent(n, slots, sems)
    loads[0].wait()
    loads[1].wait()
    width = wq.shape[1]
    row = scaled[...]
    query = inverse * jnp.dot(row, wq[...], preferred_element_type=F32)
    key = inverse * jnp.dot(row, wk[...], preferred_element_type=F32) * head_dim ** (-0.5)
    qks[me, 0] = query
    qks[me, 1] = key
    spread(n, me, qks.at[me], qks, qk_sems)
    loads[2].wait()
    loads[3].wait()
    values = inverse * dot_t(row, wv[...])
    sig_out[...] = jax.nn.sigmoid(inverse * dot_t(row, wo[...]))
    head_count = wi.shape[0]
    ingate = inverse * dot_t(row, wi[...])
    logforget = jax.nn.log_sigmoid(inverse * dot_t(row, wf[...]) + bias[...])
    eye = (
        lax.broadcasted_iota(jnp.int32, (seqs, seqs), 0)
        == lax.broadcasted_iota(jnp.int32, (seqs, seqs), 1)
    ).astype(F32)
    max_state = lax.dot_general(
        eye, max_t[...], TRANS, precision=lax.Precision.HIGHEST, preferred_element_type=F32
    )
    max_next = jnp.maximum(logforget + max_state, ingate)
    decay = jnp.exp(logforget + max_state - max_next)
    inflow = jnp.exp(ingate - max_next)
    max_out[...] = max_next
    each = wv.shape[0] // head_count
    inflow_values[...] = values * per_head(inflow, head_count, each, wv.shape[0])
    for h in range(head_count):
        decay_out[:, h * head_dim : (h + 1) * head_dim] = jnp.broadcast_to(
            decay[:, h : h + 1], (seqs, head_dim)
        )
        inflow_out[:, h * head_dim : (h + 1) * head_dim] = jnp.broadcast_to(
            inflow[:, h : h + 1], (seqs, head_dim)
        )
    relay(n, me, qks, qk_sems)
    for j in range(n):
        q_out[:, j * width : (j + 1) * width] = qks[j, 0]
        k_out[:, j * width : (j + 1) * width] = qks[j, 1]
    sent(n, qks, qk_sems)


def memory_kernel(
    q_ref,
    k_ref,
    inflow_values,
    sig,
    decay,
    inflow,
    max_ref,
    norm_ref,
    mem_hbm,
    mem_out,
    norm_out,
    gated,
    mem,
    denominators,
    in_sems,
    out_sems,
):
    seqs, head_count, each, head_dim = mem.shape
    groups = seqs // GROUP

    def chunk(g):
        return pl.ds(g * GROUP, GROUP)

    def load(g):
        return pltpu.make_async_copy(mem_hbm.at[chunk(g)], mem.at[chunk(g)], in_sems.at[g])

    def store(g):
        return pltpu.make_async_copy(mem.at[chunk(g)], mem_out.at[chunk(g)], out_sems.at[g])

    for g in range(groups):
        load(g).start()
    floor = jnp.exp(-max_ref[...])
    columns = []
    for h in range(head_count):
        span = slice(h * head_dim, (h + 1) * head_dim)
        fresh = decay[:, span] * norm_ref[:, h, :] + inflow[:, span] * k_ref[:, span]
        norm_out[:, h, :] = fresh
        mass = jnp.abs(jnp.sum(fresh * q_ref[:, span], axis=1, keepdims=True))
        columns.append(jnp.maximum(mass, floor[:, h : h + 1]))
    denominators[...] = per_head(
        jnp.concatenate(columns, axis=1), head_count, each, head_count * each
    )

    def body(g, _):
        load(g).wait()
        rows = pl.ds(pl.multiple_of(g * GROUP, GROUP), GROUP)
        lane = lax.broadcasted_iota(jnp.int32, (each, GROUP), 1)
        sides = jnp.transpose(inflow_values[rows, :])
        recalled = []
        for h in range(head_count):
            span = slice(h * head_dim, (h + 1) * head_dim)
            query, key, rate = q_ref[rows, span], k_ref[rows, span], decay[rows, span]
            found = jnp.zeros((each, GROUP), F32)
            for s in range(GROUP):
                side = sides[h * each : (h + 1) * each, s : s + 1]
                fresh = rate[s : s + 1] * mem[g * GROUP + s, h] + side * key[s : s + 1]
                mem[g * GROUP + s, h] = fresh
                total = jnp.sum(fresh * query[s : s + 1], axis=1, keepdims=True)
                found = jnp.where(lane == s, total, found)
            recalled.append(found)
        store(g).start()
        recall = jnp.transpose(jnp.concatenate(recalled, axis=0))
        gated[rows, :] = sig[rows, :] * (recall / denominators[rows, :])
        return 0

    lax.fori_loop(0, groups, body, 0)
    for g in range(groups):
        store(g).wait()


def experts_kernel(
    n_ep,
    n_tp,
    head_count,
    rows_each,
    local_experts,
    sharers,
    x_ref,
    gated,
    gain,
    mix_hbm,
    gate_hbm,
    up_hbm,
    down_hbm,
    routes_t,
    weights_t,
    out_ref,
    heads,
    own_heads,
    mix,
    gate,
    up,
    down,
    middle,
    outrows,
    inrows,
    parts,
    back,
    load_sems,
    sems,
    head_sems,
):
    ep, tp = lax.axis_index("ep"), lax.axis_index("tp")
    me = ep * n_tp + tp
    count = n_ep * n_tp
    seqs, width = x_ref.shape
    own = width // n_tp
    piece = gated.shape[1]
    peer = {"tp": lax.rem(tp + 1, n_tp)}
    blocks = gate_hbm.shape[0]
    each = piece // head_count
    head_dim = each * n_tp
    for h in range(head_count):
        for t in range(n_tp):
            pltpu.make_async_copy(
                mix_hbm.at[pl.ds(h * head_dim + t * each, each)],
                mix.at[pl.ds(t * piece + h * each, each)],
                load_sems.at[0],
            ).start()
    loads = [
        pltpu.make_async_copy(a, b, load_sems.at[i + 1])
        for i, (a, b) in enumerate(((gate_hbm, gate), (up_hbm, up), (down_hbm, down)))
    ]
    for one in loads:
        one.start()
    barrier = pltpu.get_barrier_semaphore()

    def greet(d, _):
        other = lax.rem(me + d, count)
        pl.semaphore_signal(
            barrier,
            inc=1,
            device_id={"ep": other // n_tp, "tp": lax.rem(other, n_tp)},
            device_id_type=MESH,
        )
        return 0

    lax.fori_loop(1, count, greet, 0)
    heads[tp] = gated[...].astype(BF16)
    pl.semaphore_wait(barrier, count - 1)
    spread(n_tp, tp, heads.at[tp], heads, head_sems)

    experts = local_experts * n_ep
    names = lax.broadcasted_iota(jnp.int32, (experts, seqs), 0)
    topk = routes_t.shape[0]
    chosen = [(routes_t[k : k + 1, :] == names).astype(F32) for k in range(topk)]
    earlier = (
        lax.broadcasted_iota(jnp.int32, (seqs, seqs), 0)
        < lax.broadcasted_iota(jnp.int32, (seqs, seqs), 1)
    ).astype(BF16)
    everyone = chosen[0]
    for k in range(1, topk):
        everyone = everyone + chosen[k]
    before = jnp.dot(everyone.astype(BF16), earlier, preferred_element_type=F32)
    targets = []
    for k in range(topk):
        slot = jnp.sum(chosen[k] * before, axis=0, keepdims=True).astype(jnp.int32)
        targets.append(routes_t[k : k + 1, :] * rows_each + slot)
        before = before + chosen[k]
    mine = tp // sharers
    place = lax.broadcasted_iota(jnp.int32, (n_ep * rows_each, seqs), 0)
    place = (place // rows_each * local_experts + mine) * rows_each + lax.rem(place, rows_each)
    picker = jnp.zeros(place.shape, F32)
    for k in range(topk):
        picker = picker + (place == targets[k]).astype(F32)
    picker = picker.astype(BF16)
    weight_sum = jnp.sum(weights_t[...], axis=0, keepdims=True)
    spot = lax.broadcasted_iota(jnp.int32, (count * rows_each, seqs), 0)
    source = spot // rows_each
    spot = (
        source // n_tp * local_experts + lax.rem(source, n_tp) // sharers
    ) * rows_each + lax.rem(spot, rows_each)
    combiner = jnp.zeros(spot.shape, F32)
    for k in range(topk):
        combiner = combiner + jnp.where(
            spot == targets[k], weights_t[k : k + 1, :] / weight_sum, 0.0
        )
    combiner = jnp.transpose(combiner)
    upper = combiner.astype(BF16)
    lower = (combiner - upper.astype(F32)).astype(BF16)

    relay(n_tp, tp, heads, head_sems)
    pltpu.make_async_copy(mix_hbm, mix, load_sems.at[0]).wait()
    for t in range(n_tp):
        own_heads[:, t * piece : (t + 1) * piece] = heads[t]
    flat = own_heads[...]
    total = jnp.zeros((seqs, 1), F32)
    for t in range(n_tp):
        span = slice(t * own, (t + 1) * own)
        fresh = x_ref[:, span].astype(F32) + jnp.dot(
            flat, mix[:, span], preferred_element_type=F32
        )
        fresh = fresh.astype(BF16)
        middle[:, span] = fresh
        fresh = fresh.astype(F32)
        total = total + jnp.sum(fresh * fresh, axis=1, keepdims=True)
    inverse = lax.rsqrt(total / width + eps)
    for t in range(n_tp):
        span = slice(t * own, (t + 1) * own)
        normed = (middle[:, span].astype(F32) * inverse * gain[:, span]).astype(BF16)
        picked = jnp.dot(picker, normed, preferred_element_type=F32).astype(BF16)
        outrows[:, :, span] = picked.reshape(n_ep, rows_each, own)
    for d in range(1, n_ep):
        other = lax.rem(ep + d, n_ep)
        pltpu.make_async_remote_copy(
            src_ref=outrows.at[other],
            dst_ref=inrows.at[ep],
            send_sem=sems.at[2],
            recv_sem=sems.at[3],
            device_id={"ep": other},
            device_id_type=MESH,
        ).start()
    inrows[ep] = outrows[ep]
    sent(n_tp, heads, head_sems)
    for one in loads:
        one.wait()
    there = {"ep": lax.rem(ep + 1, n_ep)}
    wait = bytes_wait(inrows.at[pl.ds(0, n_ep - 1)], sems.at[2], sems.at[3], there)
    wait.wait_recv()
    rows = inrows[...].reshape(n_ep * rows_each, width)
    hidden = []
    for b in range(blocks):
        gate_part = jnp.dot(rows, gate[b], preferred_element_type=F32)
        up_part = jnp.dot(rows, up[b], preferred_element_type=F32)
        hidden.append((jax.nn.silu(gate_part) * up_part).astype(BF16))

    def send_part(e, t):
        pltpu.make_async_remote_copy(
            src_ref=parts.at[t, e],
            dst_ref=back.at[me],
            send_sem=sems.at[4],
            recv_sem=sems.at[5],
            device_id={"ep": e, "tp": t},
            device_id_type=MESH,
        ).start()

    def finish(step, _):
        t = lax.rem(tp + 1 + step, n_tp)
        span = pl.ds(pl.multiple_of(t * own, own), own)
        result = jnp.dot(hidden[0], down[0, :, span], preferred_element_type=F32)
        for b in range(1, blocks):
            result = result + jnp.dot(hidden[b], down[b, :, span], preferred_element_type=F32)
        parts[t] = result.astype(BF16).reshape(n_ep, rows_each, own)
        for d in range(1, n_ep):
            send_part(lax.rem(ep + d, n_ep), t)

        @pl.when(step < n_tp - 1)
        def _():
            send_part(ep, t)

        return 0

    lax.fori_loop(0, n_tp, finish, 0)
    back[me] = parts[tp, ep]
    wait.wait_send()
    wait = bytes_wait(back.at[pl.ds(0, count - 1)], sems.at[4], sems.at[5], peer)
    wait.wait_recv()
    returned = back[...].reshape(count * rows_each, own)
    combined = jnp.dot(upper, returned, preferred_element_type=F32) + jnp.dot(
        lower, returned, preferred_element_type=F32
    )
    kept = middle[:, pl.ds(pl.multiple_of(tp * own, own), own)].astype(F32)
    out_ref[...] = (kept + combined).astype(BF16)
    wait.wait_send()


def local(
    n_ep,
    n_tp,
    tokens,
    mixer_gain,
    expert_gain,
    query_weight,
    key_weight,
    value_weight,
    outgate_weight,
    ingate_weight,
    forget_weight,
    forget_bias,
    mixout_weight,
    memory_state,
    norm_state,
    max_state,
    expert_gate,
    expert_up,
    expert_down,
    routes,
    route_weights,
):
    seqs, own = tokens.shape
    width = mixer_gain.shape[0]
    head_count = ingate_weight.shape[1]
    head_dim = norm_state.shape[2]
    each = value_weight.shape[2]
    piece = head_count * each
    channels = head_count * head_dim
    shape = jax.ShapeDtypeStruct
    vmem = pl.BlockSpec(memory_space=pltpu.VMEM)
    anywhere = pl.BlockSpec(memory_space=pl.ANY)
    values_t = jnp.transpose(value_weight, (1, 2, 0)).reshape(piece, width)
    outgate_t = jnp.transpose(outgate_weight, (1, 2, 0)).reshape(piece, width)
    cols = query_weight.shape[1]
    x_full, query, key, inflow_values, sig, decay, inflow, max_next = pl.pallas_call(
        functools.partial(project_kernel, n_tp, head_dim),
        out_shape=(
            shape((seqs, width), BF16),
            shape((seqs, channels), F32),
            shape((seqs, channels), F32),
            shape((seqs, piece), F32),
            shape((seqs, piece), F32),
            shape((seqs, channels), F32),
            shape((seqs, channels), F32),
            shape((seqs, head_count), F32),
        ),
        in_specs=[vmem, vmem, anywhere, anywhere, anywhere, anywhere, vmem, vmem, vmem, vmem],
        out_specs=(vmem,) * 8,
        scratch_shapes=[
            VMEM((n_tp, seqs, own), BF16),
            VMEM((n_tp, 2, seqs, cols), F32),
            VMEM((width, cols), BF16),
            VMEM((width, cols), BF16),
            VMEM((piece, width), BF16),
            VMEM((piece, width), BF16),
            VMEM((seqs, width), BF16),
            pltpu.SemaphoreType.DMA((4,)),
            pltpu.SemaphoreType.DMA((n_tp // 2 + 1,)),
            pltpu.SemaphoreType.DMA((n_tp // 2 + 1,)),
        ],
        compiler_params=pltpu.CompilerParams(
            collective_id=0, has_side_effects=True, vmem_limit_bytes=16 * 2**20
        ),
        name="project",
    )(
        tokens,
        mixer_gain.reshape(1, width),
        query_weight,
        key_weight,
        values_t,
        outgate_t,
        ingate_weight.T,
        forget_weight.T,
        forget_bias.reshape(1, head_count),
        max_state.T,
    )
    groups = seqs // GROUP
    memory_next, norm_next, gated = pl.pallas_call(
        memory_kernel,
        out_shape=(
            shape(memory_state.shape, F32),
            shape(norm_state.shape, F32),
            shape((seqs, piece), F32),
        ),
        in_specs=[vmem] * 8 + [anywhere],
        out_specs=(anywhere, vmem, vmem),
        scratch_shapes=[
            VMEM(memory_state.shape, F32),
            VMEM((seqs, piece), F32),
            pltpu.SemaphoreType.DMA((groups,)),
            pltpu.SemaphoreType.DMA((groups,)),
        ],
        compiler_params=pltpu.CompilerParams(vmem_limit_bytes=24 * 2**20),
        name="memory",
    )(query, key, inflow_values, sig, decay, inflow, max_next, norm_state, memory_state)

    block_count = expert_gate.shape[0]
    local_experts = block_count * n_tp // FF_SPLIT
    sharers = FF_SPLIT // block_count
    expert_count = local_experts * n_ep
    capacity = max(2, 2 * seqs * routes.shape[1] // expert_count)
    rows_each = -(-capacity // 16) * 16
    count = n_ep * n_tp
    mixed_out = pl.pallas_call(
        functools.partial(
            experts_kernel, n_ep, n_tp, head_count, rows_each, local_experts, sharers
        ),
        out_shape=shape((seqs, own), BF16),
        in_specs=[vmem, vmem, vmem, anywhere, anywhere, anywhere, anywhere, vmem, vmem],
        out_specs=vmem,
        scratch_shapes=[
            VMEM((n_tp, seqs, piece), BF16),
            VMEM((seqs, channels), BF16),
            VMEM(mixout_weight.shape, BF16),
            VMEM(expert_gate.shape, BF16),
            VMEM(expert_up.shape, BF16),
            VMEM(expert_down.shape, BF16),
            VMEM((seqs, width), BF16),
            VMEM((n_ep, rows_each, width), BF16),
            VMEM((n_ep, rows_each, width), BF16),
            VMEM((n_tp, n_ep, rows_each, own), BF16),
            VMEM((count, rows_each, own), BF16),
            pltpu.SemaphoreType.DMA((4,)),
            pltpu.SemaphoreType.DMA((6,)),
            pltpu.SemaphoreType.DMA((n_tp // 2 + 1,)),
        ],
        compiler_params=pltpu.CompilerParams(
            collective_id=1, has_side_effects=True, vmem_limit_bytes=40 * 2**20
        ),
        name="experts",
    )(
        x_full,
        gated,
        expert_gain.reshape(1, width),
        mixout_weight,
        expert_gate,
        expert_up,
        expert_down,
        routes.T,
        route_weights.T,
    )
    return (mixed_out, memory_next, norm_next, max_next)


def solution(mesh):
    in_specs = (
        P("ep", "tp"),
        P(),
        P(),
        P(None, "tp"),
        P(None, "tp"),
        P(None, None, "tp"),
        P(None, None, "tp"),
        P(),
        P(),
        P(),
        P(),
        P("ep", None, "tp", None),
        P("ep", None, None),
        P("ep", None),
        P(("ep", "tp"), None, None),
        P(("ep", "tp"), None, None),
        P(("ep", "tp"), None, None),
        P("ep", None),
        P("ep", None),
    )
    out_specs = (P("ep", "tp"), P("ep", None, "tp", None), P("ep", None, None), P("ep", None))
    step = functools.partial(local, mesh.shape["ep"], mesh.shape["tp"])
    return jax.shard_map(step, mesh=mesh, in_specs=in_specs, out_specs=out_specs, check_vma=False)
```

time: 187 us -> 87.1 us (0.47)
  Pallas kernels: 0 us -> 71.3 us
  blocking collectives: 59.1 us -> 0 us
  waiting for transfers between devices: 54.7 us -> 0 us
  matrix products: 28.7 us -> 0 us
  between operations: 14.4 us -> 0.76 us
  other arithmetic: 9.31 us -> 0 us
  starting transfers between devices: 7.3 us -> 0 us
    pallas_call x0 -> x3, Pallas kernels: none -> 71.3 us  [the longest x1 28.7 us: local(): pl.pallas_call(functools.partial(experts_kernel, n_ep, n_tp, head_count,...]
    all_gather x4 -> x0, blocking collectives: 59.1 us -> none  [the longest x1 16.3 us: local(): full_rows = lax.all_gather(tokens, 'tp', axis=1, tiled=True)]
    reduce_scatter x1 -> x0, waiting for transfers between devices: 35.6 us -> none  [local(): down_share = lax.psum_scatter(term, 'tp', scatter_dimension=2, tiled=True)]
    dot_general x13 -> x0, matrix products: 28.7 us -> none  [the longest x1 7.28 us: local(): jnp.einsum('shvk,shk->shv', memory_next, query_full, precision=lax.Precis...]
    all_to_all x2 -> x0, waiting for transfers between devices: 19.1 us -> none  [the longest x1 14.2 us: local(): lax.all_to_all(buffer.reshape(group_count, local_experts * capacity, norm...]
    unnamed x29 -> x40, local copies, waits for them, and re-layouts: 5.2 us -> 14 us
    all_to_all x2 -> x0, starting transfers between devices: 7.3 us -> none  [the longest x1 3.69 us: local(): lax.all_to_all(buffer.reshape(group_count, local_experts * capacity, norm...]
    add x2 -> x0, other arithmetic: 4.93 us -> none  [the longest x1 4.93 us: local(): decay_rate[:, :, None, None] * memory_state]
  transfers between devices with their start and end apart: 3 -> 0, of which waited for: 3 -> 0; matrix products, arithmetic and copies ran while one was open for 0% -> 0% of each run, Pallas kernels for 0% -> 0%
where the time goes in v1:
time: 87.1 us; the launch traced here: 86.1 us
  Pallas kernels  71.3 us (82%)
  local copies, waits for them, and re-layouts  14 us (16%)
    pallas_call x1, Pallas kernels, local(): pl.pallas_call(functools.partial(experts_kernel, n_ep, n_tp, head_count,...  28.7 us
    pallas_call x1, Pallas kernels, local(): pl.pallas_call(memory_kernel, out_shape=(shape(memory_state.shape, F32),...  23.6 us
    pallas_call x1, Pallas kernels, local(): pl.pallas_call(functools.partial(project_kernel, n_tp, head_dim), out_sha...  19 us
    unnamed x40, local copies, waits for them, and re-layouts  14 us

profile of v1, /device:TPU:0, one launch (start us, length us, event | category | flops | bytes accessed | tf_op | source)
XLA Modules:
  0.0 86.1 jit_solution(11695730103245719037)
XLA Ops:
  0.6 0.0 copy-start.5
  0.6 1.0 %copy-done.5 = bf16[2048,128]{1,0:T(8,128)(2,1)S(1)} copy-done((bf16[2048,128]{1,0:T(8,128)(2,1)S(1)}, bf16[2048,128]{1,0:T(8,128)(2,1)}, u32[]{:S(2)}) %copy-start.5) | copy-done | bytes 524312
  1.7 1.0 %copy-done.6 = bf16[2048,128]{1,0:T(8,128)(2,1)S(1)} copy-done((bf16[2048,128]{1,0:T(8,128)(2,1)S(1)}, bf16[2048,128]{1,0:T(8,128)(2,1)}, u32[]{:S(2)}) %copy-start.6) | copy-done | bytes 524312
  2.7 1.0 %copy-done.7 = bf16[2048,4,32]{0,2,1:T(8,128)(2,1)S(1)} copy-done((bf16[2048,4,32]{0,2,1:T(8,128)(2,1)S(1)}, bf16[2048,4,32]{0,2,1:T(8,128)(2,1)}, u32[]{:S(2)}) %copy-start.7) | copy-done | bytes 524312
  3.8 1.0 %copy-done.8 = bf16[2048,4,32]{0,2,1:T(8,128)(2,1)S(1)} copy-done((bf16[2048,4,32]{0,2,1:T(8,128)(2,1)S(1)}, bf16[2048,4,32]{0,2,1:T(8,128)(2,1)}, u32[]{:S(2)}) %copy-start.8) | copy-done | bytes 524312
  4.8 0.8 copy-done.10
  5.6 0.7 copy-done.11
  6.3 0.7 copy-done.12
  7.0 0.7 copy-done.13
  7.7 0.7 copy-done.15
  8.4 0.7 copy-done.18
  9.0 19.0 %project.1 = (bf16[64,2048]{1,0:T(8,128)(2,1)S(1)}, f32[64,1024]{1,0:T(8,128)S(1)}, f32[64,1024]{1,0:T(8,128)S(1)}, f32[64,128]{1,0:T(8,128)S(1)}, f32[64,128]{1...) custom-call(bf16[64,256]{1,0:T(8,128)(2,1)S(1)} %copy-done.10, ...), custom_call_target="tpu_custom_call" | custom-call | tf_op jit(solution)/shard_map/project/pallas_call | solution.py:482
  28.1 0.0 copy-start
  28.1 3.4 %copy-done = f32[64,4,32,256]{3,2,1,0:T(8,128)S(1)} copy-done((f32[64,4,32,256]{3,2,1,0:T(8,128)S(1)}, f32[64,4,32,256]{3,2,1,0:T(8,128)}, u32[]{:S(2)}) %copy-start) | copy-done | bytes 8388632
  31.4 0.9 %copy-done.9 = f32[64,4,256]{2,1,0:T(4,128)S(1)} copy-done((f32[64,4,256]{2,1,0:T(4,128)S(1)}, f32[64,4,256]{2,1,0:T(4,128)}, u32[]{:S(2)}) %copy-start.9) | copy-done | bytes 262168
  32.4 0.0 copy-start.16
  32.4 0.0 copy-start.17
  32.4 23.6 %memory.1 = (f32[64,4,32,256]{3,2,1,0:T(8,128)}, f32[64,4,256]{2,1,0:T(4,128)}, f32[64,128]{1,0:T(8,128)S(1)}) custom-call(f32[64,1024]{1,0:T(8,128)S(1)} %get-tuple-element.16.q_ref, f32[64,1024]{1,0:T(8,128)S(1)} %get-tuple-element.17.k_ref, f32[64,128]{1,0:T(8,128)S(1)} %get-tuple-element.18.inflow_values, f32[64,128]{1,0:T(8,128)S(1)} %get-tuple-element.19.sig, ...), custom_call_target="tpu_custom_call" | custom-call | tf_op jit(solution)/shard_map/memory/pallas_call | solution.py:525
  56.0 0.0 copy-done.4
  56.0 0.0 copy-done.1
  56.0 0.0 copy-done.2
  56.1 28.7 %experts.1 = bf16[64,256]{1,0:T(8,128)(2,1)S(1)} custom-call(bf16[64,2048]{1,0:T(8,128)(2,1)S(1)} %get-tuple-element.15.x_ref, f32[64,128]{1,0:T(8,128)S(1)} %get-tuple-element.23.gated, f32[1,2048]{1,0:T(1,128)S(1)} %bitcast.19, bf16[1024,2048]{1,0:T(8,128)(2,1)S(1)} %copy-done.1, bf16[2,2048,256]{2,1,0:T(8,128)(2,1)S(1)} %copy-done.2, ...), custom_call_target="tpu_custom_call" | custom-call | tf_op jit(solution)/shard_map/experts/pallas_call | solution.py:551
  84.8 0.7 copy.23
  85.4 0.6 copy.25
  (19 shorter events, 0.0 us)
Async XLA Ops:
  0.6 1.0 %copy-start.5 = (bf16[2048,128]{1,0:T(8,128)(2,1)S(1)}, bf16[2048,128]{1,0:T(8,128)(2,1)}, u32[]{:S(2)}) copy-start(bf16[2048,128]{1,0:T(8,128)(2,1)} %wq_hbm.1) | copy-start | bytes 1572868
  1.7 1.0 %copy-start.6 = (bf16[2048,128]{1,0:T(8,128)(2,1)S(1)}, bf16[2048,128]{1,0:T(8,128)(2,1)}, u32[]{:S(2)}) copy-start(bf16[2048,128]{1,0:T(8,128)(2,1)} %wk_hbm.1) | copy-start | bytes 1572868
  2.7 1.0 %copy-start.7 = (bf16[2048,4,32]{0,2,1:T(8,128)(2,1)S(1)}, bf16[2048,4,32]{0,2,1:T(8,128)(2,1)}, u32[]{:S(2)}) copy-start(bf16[2048,4,32]{0,2,1:T(8,128)(2,1)} %param.24) | copy-start | bytes 1572868
  3.8 1.0 %copy-start.8 = (bf16[2048,4,32]{0,2,1:T(8,128)(2,1)S(1)}, bf16[2048,4,32]{0,2,1:T(8,128)(2,1)}, u32[]{:S(2)}) copy-start(bf16[2048,4,32]{0,2,1:T(8,128)(2,1)} %param.25) | copy-start | bytes 1572868
  4.8 0.8 copy-start.10
  5.6 0.7 copy-start.11
  6.3 0.7 copy-start.12
  7.0 0.7 copy-start.13
  7.7 0.7 copy-start.15
  8.4 0.7 copy-start.18
  9.0 47.0 %copy-start.4 = (bf16[2,256,2048]{2,1,0:T(8,128)(2,1)S(1)}, bf16[2,256,2048]{2,1,0:T(8,128)(2,1)}, u32[]{:S(2)}) copy-start(bf16[2,256,2048]{2,1,0:T(8,128)(2,1)} %down_hbm.1) | copy-start | bytes 6291460
  28.1 3.4 %copy-start = (f32[64,4,32,256]{3,2,1,0:T(8,128)S(1)}, f32[64,4,32,256]{3,2,1,0:T(8,128)}, u32[]{:S(2)}) copy-start(f32[64,4,32,256]{3,2,1,0:T(8,128)} %mem_hbm.1) | copy-start | bytes 25165828
  31.4 0.9 %copy-start.9 = (f32[64,4,256]{2,1,0:T(4,128)S(1)}, f32[64,4,256]{2,1,0:T(4,128)}, u32[]{:S(2)}) copy-start(f32[64,4,256]{2,1,0:T(4,128)} %norm_ref.1) | copy-start | bytes 786436
  32.4 23.6 %copy-start.1 = (bf16[1024,2048]{1,0:T(8,128)(2,1)S(1)}, bf16[1024,2048]{1,0:T(8,128)(2,1)}, u32[]{:S(2)}) copy-start(bf16[1024,2048]{1,0:T(8,128)(2,1)} %mix_hbm.1) | copy-start | bytes 12582916
  32.4 23.6 %copy-start.2 = (bf16[2,2048,256]{2,1,0:T(8,128)(2,1)S(1)}, bf16[2,2048,256]{2,1,0:T(8,128)(2,1)}, u32[]{:S(2)}) copy-start(bf16[2,2048,256]{2,1,0:T(8,128)(2,1)} %gate_hbm.1) | copy-start | bytes 6291460
  32.4 23.6 %copy-start.3 = (bf16[2,2048,256]{2,1,0:T(8,128)(2,1)S(1)}, bf16[2,2048,256]{2,1,0:T(8,128)(2,1)}, u32[]{:S(2)}) copy-start(bf16[2,2048,256]{2,1,0:T(8,128)(2,1)} %up_hbm.1) | copy-start | bytes 6291460
  32.4 23.6 %copy-start.14 = (f32[2048]{0:T(1024)S(1)}, f32[2048]{0:T(1024)}, u32[]{:S(2)}) copy-start(f32[2048]{0:T(1024)} %param.21) | copy-start | bytes 24580
  32.4 23.7 %copy-start.16 = (s32[64,2]{0,1:T(2,128)S(1)}, s32[64,2]{0,1:T(2,128)}, u32[]{:S(2)}) copy-start(s32[64,2]{0,1:T(2,128)} %param.36) | copy-start | bytes 1540
  32.4 23.7 %copy-start.17 = (f32[64,2]{0,1:T(2,128)S(1)}, f32[64,2]{0,1:T(2,128)}, u32[]{:S(2)}) copy-start(f32[64,2]{0,1:T(2,128)} %param.37) | copy-start | bytes 1540

commit v2 on v1

--- a/solution.py
+++ b/solution.py
@@ -190,6 +190,7 @@
     norm_out,
     gated,
     mem,
+    held,
     denominators,
     in_sems,
     out_sems,
@@ -204,7 +205,7 @@
         return pltpu.make_async_copy(mem_hbm.at[chunk(g)], mem.at[chunk(g)], in_sems.at[g])
 
     def store(g):
-        return pltpu.make_async_copy(mem.at[chunk(g)], mem_out.at[chunk(g)], out_sems.at[g])
+        return pltpu.make_async_copy(held.at[chunk(g)], mem_out.at[chunk(g)], out_sems.at[g])
 
     for g in range(groups):
         load(g).start()
@@ -233,7 +234,7 @@
             for s in range(GROUP):
                 side = sides[h * each : (h + 1) * each, s : s + 1]
                 fresh = rate[s : s + 1] * mem[g * GROUP + s, h] + side * key[s : s + 1]
-                mem[g * GROUP + s, h] = fresh
+                held[g * GROUP + s, h] = fresh
                 total = jnp.sum(fresh * query[s : s + 1], axis=1, keepdims=True)
                 found = jnp.where(lane == s, total, found)
             recalled.append(found)
@@ -506,7 +507,7 @@
             pltpu.SemaphoreType.DMA((n_tp // 2 + 1,)),
         ],
         compiler_params=pltpu.CompilerParams(
-            collective_id=0, has_side_effects=True, vmem_limit_bytes=16 * 2**20
+            collective_id=0, has_side_effects=True
         ),
         name="project",
     )(
@@ -533,11 +534,11 @@
         out_specs=(anywhere, vmem, vmem),
         scratch_shapes=[
             VMEM(memory_state.shape, F32),
+            VMEM(memory_state.shape, F32),
             VMEM((seqs, piece), F32),
             pltpu.SemaphoreType.DMA((groups,)),
             pltpu.SemaphoreType.DMA((groups,)),
         ],
-        compiler_params=pltpu.CompilerParams(vmem_limit_bytes=24 * 2**20),
         name="memory",
     )(query, key, inflow_values, sig, decay, inflow, max_next, norm_state, memory_state)
 
@@ -572,7 +573,7 @@
             pltpu.SemaphoreType.DMA((n_tp // 2 + 1,)),
         ],
         compiler_params=pltpu.CompilerParams(
-            collective_id=1, has_side_effects=True, vmem_limit_bytes=40 * 2**20
+            collective_id=1, has_side_effects=True
         ),
         name="experts",
     )(

time: 87.1 us -> 73.9 us (0.85)
  local copies, waits for them, and re-layouts: 14 us -> 2.03 us
  Pallas kernels: 71.3 us -> 70.4 us
    unnamed x40 -> x4, local copies, waits for them, and re-layouts: 14 us -> 2.03 us
    pallas_call x1, Pallas kernels: 28.7 us -> 24.5 us  [local(): pl.pallas_call(functools.partial(experts_kernel, n_ep, n_tp, head_count,...]
    pallas_call x1, Pallas kernels: 19 us -> 20.8 us  [local(): pl.pallas_call(functools.partial(project_kernel, n_tp, head_dim), out_sha...]
    pallas_call x1, Pallas kernels: 23.6 us -> 25.2 us  [local(): pl.pallas_call(memory_kernel, out_shape=(shape(memory_state.shape, F32),...]
where the time goes in v2:
time: 73.9 us; the launch traced here: 73.2 us
  Pallas kernels  70.4 us (95%)
  local copies, waits for them, and re-layouts  2.03 us (3%)
    pallas_call x1, Pallas kernels, local(): pl.pallas_call(memory_kernel, out_shape=(shape(memory_state.shape, F32),...  25.2 us
    pallas_call x1, Pallas kernels, local(): pl.pallas_call(functools.partial(experts_kernel, n_ep, n_tp, head_count,...  24.5 us
    pallas_call x1, Pallas kernels, local(): pl.pallas_call(functools.partial(project_kernel, n_tp, head_dim), out_sha...  20.8 us
    unnamed x4, local copies, waits for them, and re-layouts  2.03 us

profile of v2, /device:TPU:0, one launch (start us, length us, event | category | flops | bytes accessed | tf_op | source)
XLA Modules:
  0.0 73.2 jit_solution(13159597965607700637)
XLA Ops:
  0.6 20.8 %project.1 = (bf16[64,2048]{1,0:T(8,128)(2,1)}, f32[64,1024]{1,0:T(8,128)}, f32[64,1024]{1,0:T(8,128)}, f32[64,128]{1,0:T(8,128)}, f32[64,128]{1,0:T(8,128)}, /*...) custom-call(bf16[64,256]{1,0:T(8,128)(2,1)} %tok.1, f32[1,2048]{1,0:T(1,128)} %bitcast.18, ...), custom_call_target="tpu_custom_call" | custom-call | tf_op jit(solution)/shard_map/project/pallas_call | solution.py:483
  21.4 25.2 %memory.1 = (f32[64,4,32,256]{3,2,1,0:T(8,128)}, f32[64,4,256]{2,1,0:T(4,128)}, f32[64,128]{1,0:T(8,128)}) custom-call(f32[64,1024]{1,0:T(8,128)} %get-tuple-element.16.q_ref, f32[64,1024]{1,0:T(8,128)} %get-tuple-element.17.k_ref, f32[64,128]{1,0:T(8,128)} %get-tuple-element.18.inflow_values, f32[64,128]{1,0:T(8,128)} %get-tuple-element.19.sig, ...), custom_call_target="tpu_custom_call" | custom-call | tf_op jit(solution)/shard_map/memory/pallas_call | solution.py:526
  46.6 0.0 copy-start
  46.6 24.5 %experts.1 = bf16[64,256]{1,0:T(8,128)(2,1)} custom-call(bf16[64,2048]{1,0:T(8,128)(2,1)} %get-tuple-element.15.x_ref, f32[64,128]{1,0:T(8,128)} %get-tuple-element.23.gated, f32[1,2048]{1,0:T(1,128)} %bitcast.19, bf16[1024,2048]{1,0:T(8,128)(2,1)} %mix_hbm.1, bf16[2,2048,256]{2,1,0:T(8,128)(2,1)} %gate_hbm.1, bf16[2,2048,256]{2,1,0:T(8,128)(2,1)} %up_hbm.1, ...), custom_call_target="tpu_custom_call" | custom-call | tf_op jit(solution)/shard_map/experts/pallas_call | solution.py:552
  71.1 0.0 copy-done
  71.1 0.7 copy.23
  71.8 1.4 %copy.25 = bf16[64,256]{1,0:T(8,128)(2,1)} copy(bf16[64,256]{1,0:T(8,128)(2,1)} %experts.1) | data formatting | bytes 65536
Async XLA Ops:
  46.6 24.5 %copy-start = (f32[64,4]{1,0:T(8,128)S(1)}, f32[64,4]{1,0:T(8,128)}, u32[]{:S(2)}) copy-start(f32[64,4]{1,0:T(8,128)} %get-tuple-element.29.max_ref) | copy-start | bytes 3076
